TPU v7x, 32 devices: a whole 2x2x4 slice. The times are simulated.
32 devices in a mesh: dp: 4 (over y, x), kv: 4 (over z), tp: 2 (over core).
Axes of the slice: x: 2, y: 2, z: 4, core: 2. Of those that a mesh axis runs over, the one named last changes fastest.
Arguments:
- tokens: bfloat16 [256, 2048], P('dp', ('kv', 'tp')), parts along dimension 0, may hold values from -64 to 64, as said below
- lengths: int32 [32], P(('dp', 'kv', 'tp')), parts along dimension 0, may hold values from 1 to 8, 28 in all
- state: float32 [32, 16, 128, 128], P(('dp', 'kv', 'tp')), parts along dimension 0, may hold values from -1.8 to 1.8
- gain_first: float32 [2048], replicated, may hold values from 0.1 to 1.9
- first_gate: bfloat16 [2048, 5632], P(None, 'kv'), may hold values from -0.125 to 0.125
- first_up: bfloat16 [2048, 5632], P(None, 'kv'), may hold values from -0.125 to 0.125
- first_down: bfloat16 [5632, 2048], P('kv'), may hold values from -0.109375 to 0.109375
- gain_mix: float32 [2048], replicated, may hold values from 0.1 to 1.9
- query_weight: bfloat16 [2048, 2048], P(None, ('kv', 'tp')), may hold values from -0.125 to 0.125
- key_weight: bfloat16 [2048, 2048], P(None, ('kv', 'tp')), may hold values from -0.125 to 0.125
- value_weight: bfloat16 [2048, 2048], P(None, ('kv', 'tp')), may hold values from -0.125 to 0.125
- gating_weight: bfloat16 [2048, 2048], P(None, ('kv', 'tp')), may hold values from -0.125 to 0.125
- write_weight: bfloat16 [2048, 16], replicated, may hold values from -0.125 to 0.125
- forget_weight: bfloat16 [2048, 16], replicated, may hold values from -0.125 to 0.125
- forget_rate: float32 [16], replicated, may hold values from -4 to 1.5
- out_weight: bfloat16 [2048, 2048], P(None, ('kv', 'tp')), may hold values from -0.125 to 0.125
- gain_second: float32 [2048], replicated, may hold values from 0.1 to 1.9
- second_gate: bfloat16 [2048, 5632], P(None, 'kv'), may hold values from -0.125 to 0.125
- second_up: bfloat16 [2048, 5632], P(None, 'kv'), may hold values from -0.125 to 0.125
- second_down: bfloat16 [5632, 2048], P('kv'), may hold values from -0.109375 to 0.109375
Outputs:
- mixed_out: bfloat16 [256, 2048], P('dp', ('kv', 'tp')), parts along dimension 0
- new_state: float32 [32, 16, 128, 128], P(('dp', 'kv', 'tp')), parts along dimension 0
There are 4 independent parts, one for each index of `dp`. A program takes and returns all parts, laid end to end along the dimension named above; an argument that names none is the same for every part. Nothing has to cross between parts.
Inputs may be any that keep to these rules, and one draw needn't show every extreme that they name: Activations of the new tokens. `lengths`: the live new tokens of each sequence; within each independent group of 8 sequences (one part along dp) they sum to seven halves of 8, rounded down, and some sequence of each group has all 8 live.
All inputs are finite; a program needn't handle non-finite values.
Results may differ from a plain program's by a relative error of at most 0.0058.
Values may be sent and summed in bfloat16 or wider, within the bound.
A program may use at most 128 MiB of HBM per device.

v0:
```python
import math
import jax
import jax.numpy as jnp
from jax import lax
from jax.sharding import PartitionSpec as P

HEADS = 16
HEAD = 128
BLK = 8
EPSILON = 1e-06


def fold_step(gain, gate_cols, up_cols, portion):
    values = portion.astype(jnp.float32)
    scaled = (values * gain).astype(jnp.bfloat16)
    gate_acc = jnp.dot(scaled, gate_cols, preferred_element_type=jnp.float32)
    up_acc = jnp.dot(scaled, up_cols, preferred_element_type=jnp.float32)
    squares = jnp.sum(values * values, axis=1)
    return (gate_acc, up_acc, squares)


def finish_units(gate_acc, up_acc, squares, channels, down_rows):
    row_scale = lax.rsqrt(squares / channels + EPSILON)[:, None]
    hidden = (jax.nn.silu(gate_acc * row_scale) * (up_acc * row_scale)).astype(jnp.bfloat16)
    return jnp.dot(hidden, down_rows, preferred_element_type=jnp.float32)


def feed_forward(hidden_in, gain, w_gate, w_up, w_down):
    channels = gain.shape[0]
    paired = lax.all_to_all(hidden_in, "tp", split_axis=0, concat_axis=1, tiled=True)
    gate_acc, up_acc, squares = fold_step(
        gain, w_gate, w_up, lax.all_gather(paired, "kv", axis=1, tiled=True)
    )
    ffn_term = finish_units(gate_acc, up_acc, squares, channels, w_down)
    partial_value = lax.psum_scatter(ffn_term, "kv", scatter_dimension=1, tiled=True)
    summed = lax.all_to_all(partial_value, "tp", split_axis=1, concat_axis=0, tiled=True)
    return (hidden_in.astype(jnp.float32) + 0.5 * summed).astype(jnp.bfloat16)


def delta_block(query, key_in, value, gating, write_pre, forget_pre, rates, live, state):
    seq_count, block_len, head_count, head_size = query.shape
    precise = lax.Precision.HIGHEST
    query_unit = (
        query
        * lax.rsqrt(jnp.sum(query * query, axis=-1, keepdims=True) + EPSILON)
        / math.sqrt(head_size)
    )
    key_unit = key_in * lax.rsqrt(jnp.sum(key_in * key_in, axis=-1, keepdims=True) + EPSILON)
    live_rows = live[:, :, None]
    write_gate = jax.nn.sigmoid(write_pre) * live_rows
    forget = -jnp.exp(rates)[None, None, :] * jax.nn.softplus(forget_pre) * live_rows
    cumulative = jnp.cumsum(forget, axis=1)
    cum_heads = jnp.transpose(cumulative, (0, 2, 1))
    positions = jnp.arange(block_len)
    causal = positions[:, None] >= positions[None, :]
    strict = positions[:, None] > positions[None, :]
    differ = jnp.minimum(cum_heads[:, :, :, None] - cum_heads[:, :, None, :], 0.0)
    decay_mat = jnp.where(causal, jnp.exp(differ), 0.0)
    key_dots = jnp.einsum("sthd,suhd->shtu", key_unit, key_unit, precision=precise)
    write_heads = jnp.transpose(write_gate, (0, 2, 1))
    strict_part = jnp.where(strict, write_heads[:, :, :, None] * decay_mat * key_dots, 0.0)
    identity = jnp.eye(block_len, dtype=jnp.float32)
    squared = jnp.einsum("shtu,shuv->shtv", strict_part, strict_part, precision=precise)
    fourth = jnp.einsum("shtu,shuv->shtv", squared, squared, precision=precise)
    inverse = jnp.einsum(
        "shtu,shuv->shtv", identity - strict_part, identity + squared, precision=precise
    )
    inverse = jnp.einsum("shtu,shuv->shtv", inverse, identity + fourth, precision=precise)
    growth = jnp.exp(cumulative)
    target = jnp.einsum(
        "shtu,suhv->sthv", inverse, write_gate[..., None] * value, precision=precise
    )
    key_mix = jnp.einsum(
        "shtu,suhk->sthk", inverse, (write_gate * growth)[..., None] * key_unit, precision=precise
    )
    update = target - jnp.einsum("sthk,shkv->sthv", key_mix, state, precision=precise)
    scores = jnp.einsum("sthd,suhd->shtu", query_unit, key_unit, precision=precise) * decay_mat
    attend = jnp.einsum("sthk,shkv->sthv", query_unit * growth[..., None], state, precision=precise)
    attend = attend + jnp.einsum("shtu,suhv->sthv", scores, update, precision=precise)
    final_cum = cumulative[:, -1:, :]
    fading = jnp.exp(final_cum - cumulative)
    new_state = jnp.exp(final_cum[:, 0, :])[:, :, None, None] * state
    new_state = new_state + jnp.einsum(
        "sthk,sthv->shkv", key_unit * fading[..., None], update, precision=precise
    )
    normed = attend * lax.rsqrt(jnp.mean(attend * attend, axis=-1, keepdims=True) + EPSILON)
    normed = normed * jax.nn.silu(gating) * live[:, :, None, None]
    mixed_heads = normed.reshape(seq_count * block_len, head_count * head_size).astype(jnp.bfloat16)
    return (mixed_heads, new_state)


def per_device(
    tokens,
    lengths,
    state,
    gain_first,
    first_gate,
    first_up,
    first_down,
    gain_mix,
    query_weight,
    key_weight,
    value_weight,
    gating_weight,
    write_weight,
    forget_weight,
    forget_rate,
    out_weight,
    gain_second,
    second_gate,
    second_up,
    second_down,
):
    after_first = feed_forward(tokens, gain_first, first_gate, first_up, first_down)
    seq_count = lengths.shape[0]
    own_count = seq_count * BLK
    whole_rows = lax.all_gather(after_first, ("kv", "tp"), axis=1, tiled=True)
    scaled_all = (whole_rows.astype(jnp.float32) * gain_mix).astype(jnp.bfloat16)
    stacked = jnp.stack(
        [
            jnp.dot(scaled_all, matrix, preferred_element_type=jnp.float32)
            for matrix in (query_weight, key_weight, value_weight, gating_weight)
        ]
    )
    owned = lax.all_to_all(
        stacked.astype(jnp.bfloat16), ("kv", "tp"), split_axis=1, concat_axis=2, tiled=True
    ).astype(stacked.dtype)
    row_start = lax.axis_index(("kv", "tp")) * own_count
    own_values = lax.dynamic_slice_in_dim(whole_rows, row_start, own_count, 0).astype(jnp.float32)
    own_scaled = lax.dynamic_slice_in_dim(scaled_all, row_start, own_count, 0)
    mix_scale = lax.rsqrt(jnp.mean(own_values * own_values, axis=1, keepdims=True) + EPSILON)
    query = (owned[0] * mix_scale).reshape(seq_count, BLK, HEADS, HEAD)
    key_in = (owned[1] * mix_scale).reshape(seq_count, BLK, HEADS, HEAD)
    value = (owned[2] * mix_scale).reshape(seq_count, BLK, HEADS, HEAD)
    gating = (owned[3] * mix_scale).reshape(seq_count, BLK, HEADS, HEAD)
    write_pre = (
        jnp.dot(own_scaled, write_weight, preferred_element_type=jnp.float32) * mix_scale
    ).reshape(seq_count, BLK, HEADS)
    forget_pre = (
        jnp.dot(own_scaled, forget_weight, preferred_element_type=jnp.float32) * mix_scale
    ).reshape(seq_count, BLK, HEADS)
    positions = jnp.arange(BLK, dtype=jnp.int32)
    live = (positions[None, :] < lengths[:, None]).astype(jnp.float32)
    mixed_heads, new_state = delta_block(
        query, key_in, value, gating, write_pre, forget_pre, forget_rate, live, state
    )
    half_cols = mixed_heads.shape[1] // 2
    portion = lax.all_gather(mixed_heads, ("kv", "tp"), axis=0, tiled=True)
    first_half = jnp.dot(
        portion[:, :half_cols], out_weight[:half_cols], preferred_element_type=jnp.float32
    ).astype(jnp.bfloat16)
    second_half = jnp.dot(
        portion[:, half_cols:], out_weight[half_cols:], preferred_element_type=jnp.float32
    ).astype(jnp.bfloat16)
    first_half, second_half = lax.optimization_barrier((first_half, second_half))
    mixed_sum = first_half.astype(jnp.float32) + second_half.astype(jnp.float32)
    after_mix = (after_first.astype(jnp.float32) + mixed_sum).astype(jnp.bfloat16)
    mixed_out = feed_forward(after_mix, gain_second, second_gate, second_up, second_down)
    return (mixed_out, new_state)


def solution(mesh):
    in_specs = (
        P("dp", ("kv", "tp")),
        P(("dp", "kv", "tp")),
        P(("dp", "kv", "tp"), None, None, None),
        P(),
        P(None, "kv"),
        P(None, "kv"),
        P("kv", None),
        P(),
        P(None, ("kv", "tp")),
        P(None, ("kv", "tp")),
        P(None, ("kv", "tp")),
        P(None, ("kv", "tp")),
        P(),
        P(),
        P(),
        P(None, ("kv", "tp")),
        P(),
        P(None, "kv"),
        P(None, "kv"),
        P("kv", None),
    )
    out_specs = (P("dp", ("kv", "tp")), P(("dp", "kv", "tp"), None, None, None))
    return jax.shard_map(
        per_device, mesh=mesh, in_specs=in_specs, out_specs=out_specs, check_vma=False
    )
```

profile of v0, /device:TPU:0, one launch (start us, length us, event | category | flops | bytes accessed | tf_op | source)
XLA Modules:
  0.0 174.8 jit_solution(16179178874863830319)
XLA Ops:
  7.2 4.8 %all_to_all.73 = bf16[2,32,256]{2,1,0:T(8,128)(2,1)S(1)} all-to-all(bf16[2,32,256]{2,1,0:T(8,128)(2,1)} %bitcast.150), channel_id=1, replica_groups=mesh['dp'=4,'kv'=4,'tp'=2] {'tp'}, dimensions={0} | all-to-all | bytes 65536 | tf_op jit(solution)/shard_map/all_to_all | solution.py:30
  12.0 15.1 %all_gather.12 = bf16[32,2048]{1,0:T(8,128)(2,1)S(1)} all-gather(bf16[32,512]{1,0:T(8,128)(2,1)S(1)} %bitcast.146), channel_id=1, replica_groups=mesh['dp'=4,'kv'=4,'tp'=2] {'kv'}, dimensions={1}, use_global_device_ids=true | all-gather | bytes 163840 | tf_op jit(solution)/shard_map/all_gather | solution.py:32
  27.2 3.7 %convolution_multiply_fusion.3 = f32[32,1408]{1,0:T(8,128)S(1)} fusion(bf16[2048,1408]{1,0:T(8,128)(2,1)} %param.24, bf16[32,2048]{1,0:T(8,128)(2,1)S(1)} %all_gather.12, f32[2048]{0:T(1024)} %param.23, f32[32]{0:T(128)S(1)} %add_rsqrt_fusion.5), kind=kOutput, calls=%fused_computation.5 | convolution fusion | flops 184791040 | bytes 6086784 | tf_op jit(solution)/shard_map/dot_general | solution.py:16
  31.0 7.1 %fusion.21 = f32[32,2048]{1,0:T(8,128)} fusion(bf16[1408,2048]{1,0:T(8,128)(2,1)} %param.26, bf16[2048,1408]{1,0:T(8,128)(2,1)} %param.25, f32[32,1408]{1,0:T(8,128)S(1)} %convolution_multiply_fusion.3, bf16[32,2048]{1,0:T(8,128)(2,1)S(1)} %all_gather.12, f32[2048]{0:T(1024)S(1)} %copy-done.4, f32[32]{0:T(128)S(1)} %add_rsqrt_fusion.5), kind=kOutput, calls=%fused_computation.41 | convolution fusion | flops 369610752 | bytes 12116096 | tf_op jit(solution)/shard_map/dot_general | solution.py:25
  38.9 20.5 %reduce-scatter.3.cloned.1.call-done = f32[32,512]{1,0:T(8,128)} async-done(((f32[32,2048]{1,0:T(8,128)}), f32[32,512]{1,0:T(8,128)}) %reduce-scatter.3.cloned.1.call-update) | async-done | bytes 65552 | tf_op jit(solution)/shard_map/reduce_scatter | solution.py:35
  60.2 3.8 %all_to_all.74 = f32[32,2,256]{2,0,1:T(8,128)S(1)} all-to-all(f32[32,2,256]{2,0,1:T(8,128)S(1)} %bitcast.144), channel_id=1, replica_groups=mesh['dp'=4,'kv'=4,'tp'=2] {'tp'}, dimensions={1} | all-to-all | bytes 131072 | tf_op jit(solution)/shard_map/all_to_all | solution.py:36
  64.0 14.3 %all_gather.13 = bf16[64,2048]{1,0:T(8,128)(2,1)S(1)} all-gather(bf16[64,256]{1,0:T(8,128)(2,1)S(1)} %fusion.51), channel_id=1, replica_groups=mesh['dp'=4,'kv'=4,'tp'=2] {'kv','tp'}, dimensions={1}, use_global_device_ids=true | all-gather | bytes 294912 | tf_op jit(solution)/shard_map/all_gather | solution.py:117
  79.2 1.5 fusion.10
  80.7 1.5 fusion.9
  83.0 3.4 %all-to-all-start.2 = ((bf16[4,64,256]{2,0,1:T(4,128)(2,1)}), bf16[4,64,256]{2,0,1:T(4,128)(2,1)S(1)}, u32[]{:S(2)}, u32[]{:S(2)}) async-start(bf16[4,64,256]{2,0,1:T(4,128)(2,1)} %copy.99), calls=%async_computation.3 | async-start | bytes 262144 | tf_op jit(solution)/shard_map/all_to_all | solution.py:125
  86.7 0.9 fusion.80
  87.8 5.3 %all-to-all-done.2 = bf16[4,64,256]{2,0,1:T(4,128)(2,1)S(1)} async-done(((bf16[4,64,256]{2,0,1:T(4,128)(2,1)}), bf16[4,64,256]{2,0,1:T(4,128)(2,1)S(1)}, u32[]{:S(2)}, u32[]{:S(2)}) %all-to-all-start.2) | async-done | bytes 131104 | tf_op jit(solution)/shard_map/all_to_all | solution.py:125
  96.0 1.0 convolution_bitcast_fusion.3
  96.9 1.0 fusion.7
  98.5 14.2 %all_gather.14 = bf16[64,2048]{1,0:T(8,128)(2,1)S(1)} all-gather(bf16[8,2048]{1,0:T(8,128)(2,1)S(1)} %fusion.70), channel_id=1, replica_groups=mesh['dp'=4,'kv'=4,'tp'=2] {'kv','tp'}, dimensions={0}, use_global_device_ids=true | all-gather | bytes 294912 | tf_op jit(solution)/shard_map/all_gather | solution.py:148
  112.8 1.2 convolution_convert_fusion
  114.0 1.2 convolution_convert_fusion.1
  115.3 3.7 %all_to_all.75 = bf16[2,32,256]{2,1,0:T(8,128)(2,1)S(1)} all-to-all(bf16[2,32,256]{2,1,0:T(8,128)(2,1)S(1)} %bitcast.143), channel_id=1, replica_groups=mesh['dp'=4,'kv'=4,'tp'=2] {'tp'}, dimensions={0} | all-to-all | bytes 65536 | tf_op jit(solution)/shard_map/all_to_all | solution.py:30
  119.0 13.6 %all_gather.15 = bf16[32,2048]{1,0:T(8,128)(2,1)S(1)} all-gather(bf16[32,512]{1,0:T(8,128)(2,1)S(1)} %bitcast.147), channel_id=1, replica_groups=mesh['dp'=4,'kv'=4,'tp'=2] {'kv'}, dimensions={1}, use_global_device_ids=true | all-gather | bytes 163840 | tf_op jit(solution)/shard_map/all_gather | solution.py:32
  132.7 3.6 %convolution_multiply_fusion.1 = f32[32,1408]{1,0:T(8,128)S(1)} fusion(bf16[2048,1408]{1,0:T(8,128)(2,1)} %param.37, bf16[32,2048]{1,0:T(8,128)(2,1)S(1)} %all_gather.15, f32[2048]{0:T(1024)S(1)} %copy-done.5, f32[32]{0:T(128)S(1)} %add_rsqrt_fusion.3), kind=kOutput, calls=%fused_computation.2 | convolution fusion | flops 184791040 | bytes 6086784 | tf_op jit(solution)/shard_map/dot_general | solution.py:16
  136.4 7.0 %fusion.20 = f32[32,2048]{1,0:T(8,128)} fusion(bf16[1408,2048]{1,0:T(8,128)(2,1)} %param.39, bf16[2048,1408]{1,0:T(8,128)(2,1)} %param.38, f32[32,1408]{1,0:T(8,128)S(1)} %convolution_multiply_fusion.1, bf16[32,2048]{1,0:T(8,128)(2,1)S(1)} %all_gather.15, f32[2048]{0:T(1024)S(1)} %copy-done.5, f32[32]{0:T(128)S(1)} %add_rsqrt_fusion.3), kind=kOutput, calls=%fused_computation.40 | convolution fusion | flops 369610752 | bytes 12116096 | tf_op jit(solution)/shard_map/dot_general | solution.py:25
  143.5 2.8 %fusion.4 = f32[1,16,128,128]{3,2,1,0:T(8,128)} fusion(f32[8,16,128]{2,0,1:T(8,128)S(1)} %fusion.7, f32[1,16,128,128]{3,2,1,0:T(8,128)S(1)} %copy-done.1, f32[16]{0:T(128)S(1)} %fusion.86, f32[8,16,128]{2,1,0:T(8,128)S(1)} %get-tuple-element.20), kind=kOutput, calls=%fused_computation.9 | convolution fusion | flops 25690112 | bytes 2228288 | tf_op jit(solution)/shard_map/sthk,sthv->shkv/dot_general | solution.py:83
  146.3 16.4 %reduce-scatter.5.cloned.1.call-done = f32[32,512]{1,0:T(8,128)} async-done(((f32[32,2048]{1,0:T(8,128)}), f32[32,512]{1,0:T(8,128)}) %reduce-scatter.5.cloned.1.call-update) | async-done | bytes 65552 | tf_op jit(solution)/shard_map/reduce_scatter | solution.py:35
  163.6 3.8 %all_to_all.76 = f32[32,2,256]{2,0,1:T(8,128)S(1)} all-to-all(f32[32,2,256]{2,0,1:T(8,128)S(1)} %bitcast.145), channel_id=1, replica_groups=mesh['dp'=4,'kv'=4,'tp'=2] {'tp'}, dimensions={1} | all-to-all | bytes 131072 | tf_op jit(solution)/shard_map/all_to_all | solution.py:36
  (79 shorter events, 8.1 us)
Async XLA Ops:
  7.2 71.4 %copy-start = (bf16[2048,256]{1,0:T(8,128)(2,1)S(1)}, bf16[2048,256]{1,0:T(8,128)(2,1)}, u32[]{:S(2)}) copy-start(bf16[2048,256]{1,0:T(8,128)(2,1)} %param.31) | copy-start | bytes 3145732
  7.2 23.7 %copy-start.4 = (f32[2048]{0:T(1024)S(1)}, f32[2048]{0:T(1024)}, u32[]{:S(2)}) copy-start(f32[2048]{0:T(1024)} %param.23) | copy-start | bytes 24580
  7.2 52.2 %reduce-scatter.3.cloned.1.call-start = ((), (), s32[]{:S(2)}) async-start(), calls=%async_computation.7 | async-start | bytes 327680 | tf_op jit(solution)/shard_map/reduce_scatter | solution.py:35
  30.9 7.9 %copy-start.8 = (f32[16]{0:T(128)S(1)}, f32[16]{0:T(128)}, u32[]{:S(2)}) copy-start(f32[16]{0:T(128)} %param.34) | copy-start | bytes 196
  30.9 33.1 %copy-start.3 = (bf16[64,256]{1,0:T(8,128)(2,1)S(1)}, bf16[64,256]{1,0:T(8,128)(2,1)}, u32[]{:S(2)}) copy-start(bf16[64,256]{1,0:T(8,128)(2,1)} %param.20) | copy-start | bytes 98308
  30.9 47.6 %copy-start.6 = (f32[2048]{0:T(1024)S(1)}, f32[2048]{0:T(1024)}, u32[]{:S(2)}) copy-start(f32[2048]{0:T(1024)} %param.27) | copy-start | bytes 24580
  30.9 47.9 %copy-start.2 = (bf16[2048,256]{1,0:T(8,128)(2,1)S(1)}, bf16[2048,256]{1,0:T(8,128)(2,1)}, u32[]{:S(2)}) copy-start(bf16[2048,256]{1,0:T(8,128)(2,1)} %param.30) | copy-start | bytes 3145732
  38.1 48.4 %copy-start.7 = (bf16[2048,16]{0,1:T(8,128)(2,1)S(1)}, bf16[2048,16]{0,1:T(8,128)(2,1)}, u32[]{:S(2)}) copy-start(bf16[2048,16]{0,1:T(8,128)(2,1)} %param.33) | copy-start | bytes 196612
  64.0 31.9 %copy-start.1 = (f32[1,16,128,128]{3,2,1,0:T(8,128)S(1)}, f32[1,16,128,128]{3,2,1,0:T(8,128)}, u32[]{:S(2)}) copy-start(f32[1,16,128,128]{3,2,1,0:T(8,128)} %param.22) | copy-start | bytes 3145732
  80.7 52.0 %copy-start.5 = (f32[2048]{0:T(1024)S(1)}, f32[2048]{0:T(1024)}, u32[]{:S(2)}) copy-start(f32[2048]{0:T(1024)} %param.36) | copy-start | bytes 24580
  83.0 10.1 %all-to-all-start.2 = ((bf16[4,64,256]{2,0,1:T(4,128)(2,1)}), bf16[4,64,256]{2,0,1:T(4,128)(2,1)S(1)}, u32[]{:S(2)}, u32[]{:S(2)}) async-start(bf16[4,64,256]{2,0,1:T(4,128)(2,1)} %copy.99), calls=%async_computation.3 | async-start | bytes 262144 | tf_op jit(solution)/shard_map/all_to_all | solution.py:125
  86.4 76.3 %reduce-scatter.5.cloned.1.call-start = ((), (), s32[]{:S(2)}) async-start(), calls=%async_computation.8 | async-start | bytes 327680 | tf_op jit(solution)/shard_map/reduce_scatter | solution.py:35
Sparse Core Ops, SparseCore 0:
  38.2 21.0 reduce-scatter.2
  143.6 19.1 reduce-scatter.4
where the time goes:
time: 176 us; the launch traced here: 175 us
  blocking collectives  73.2 us (42%)
  waiting for transfers between devices  42.3 us (24%)
  matrix products  35.8 us (20%)
  between operations  15.2 us (9%)
  starting transfers between devices  3.45 us (2%)
  local copies, waits for them, and re-layouts  3.13 us (2%)
  other arithmetic  1.76 us (1%)
    reduce_scatter x2, waiting for transfers between devices, feed_forward(): lax.psum_scatter(ffn_term, 'kv', scatter_dimension=1, tiled=True)  36.9 us
    all_gather x2, blocking collectives, feed_forward(): lax.all_gather(paired, 'kv', axis=1, tiled=True)  28.6 us
    all_gather x1, blocking collectives, per_device(): whole_rows = lax.all_gather(after_first, ('kv', 'tp'), axis=1, tiled=True)  14.3 us
    all_gather x1, blocking collectives, per_device(): portion = lax.all_gather(mixed_heads, ('kv', 'tp'), axis=0, tiled=True)  14.2 us
    dot_general x2, matrix products, finish_units(): return jnp.dot(hidden, down_rows, preferred_element_type=jnp.float32)  14.2 us
    all_to_all x2, blocking collectives, feed_forward(): lax.all_to_all(hidden_in, 'tp', split_axis=0, concat_axis=1, tiled=True)  8.52 us
    all_to_all x2, blocking collectives, feed_forward(): lax.all_to_all(partial_value, 'tp', split_axis=1, concat_axis=0, tiled=True)  7.56 us
    dot_general x2, matrix products, fold_step(): gate_acc = jnp.dot(scaled, gate_cols, preferred_element_type=jnp.float32)  7.31 us
  transfers between devices with their start and end apart: 3, of which 3 were waited for; matrix products, arithmetic and copies ran while one was open for 2% of the time, Pallas kernels for 0%

commit v1 on v0

--- a/solution.py
+++ b/solution.py
@@ -33,7 +33,9 @@
     )
     ffn_term = finish_units(gate_acc, up_acc, squares, channels, w_down)
     partial_value = lax.psum_scatter(ffn_term, "kv", scatter_dimension=1, tiled=True)
-    summed = lax.all_to_all(partial_value, "tp", split_axis=1, concat_axis=0, tiled=True)
+    cells = jnp.split(partial_value, lax.axis_size("tp"), axis=1)
+    received = lax.all_to_all(jnp.stack(cells), "tp", 0, 0)
+    summed = jnp.concatenate(received, axis=0)
     return (hidden_in.astype(jnp.float32) + 0.5 * summed).astype(jnp.bfloat16)
 
 

time: 176 us -> 176 us (level)
  no operation moved by 1% of the time
where the time goes in v1:
time: 176 us; the launch traced here: 175 us
  blocking collectives  73.3 us (42%)
  waiting for transfers between devices  42.2 us (24%)
  matrix products  35.8 us (20%)
  between operations  15.2 us (9%)
  starting transfers between devices  3.45 us (2%)
  local copies, waits for them, and re-layouts  3 us (2%)
  other arithmetic  1.77 us (1%)
    reduce_scatter x2, waiting for transfers between devices, feed_forward(): lax.psum_scatter(ffn_term, 'kv', scatter_dimension=1, tiled=True)  36.9 us
    all_gather x2, blocking collectives, feed_forward(): lax.all_gather(paired, 'kv', axis=1, tiled=True)  28.6 us
    all_gather x1, blocking collectives, per_device(): whole_rows = lax.all_gather(after_first, ('kv', 'tp'), axis=1, tiled=True)  14.3 us
    all_gather x1, blocking collectives, per_device(): portion = lax.all_gather(mixed_heads, ('kv', 'tp'), axis=0, tiled=True)  14.2 us
    dot_general x2, matrix products, finish_units(): return jnp.dot(hidden, down_rows, preferred_element_type=jnp.float32)  14.2 us
    all_to_all x2, blocking collectives, feed_forward(): lax.all_to_all(hidden_in, 'tp', split_axis=0, concat_axis=1, tiled=True)  8.52 us
    all_to_all x2, blocking collectives, feed_forward(): received = lax.all_to_all(jnp.stack(cells), 'tp', 0, 0)  7.58 us
    dot_general x2, matrix products, fold_step(): gate_acc = jnp.dot(scaled, gate_cols, preferred_element_type=jnp.float32)  7.31 us
  transfers between devices with their start and end apart: 3, of which 3 were waited for; matrix products, arithmetic and copies ran while one was open for 2% of the time, Pallas kernels for 0%

profile of v1, /device:TPU:0, one launch (start us, length us, event | category | flops | bytes accessed | tf_op | source)
XLA Modules:
  0.0 174.7 jit_solution(2432774181499316795)
XLA Ops:
  7.2 4.8 %all_to_all.57 = bf16[2,32,256]{2,1,0:T(8,128)(2,1)S(1)} all-to-all(bf16[2,32,256]{2,1,0:T(8,128)(2,1)} %bitcast.144), channel_id=1, replica_groups=mesh['dp'=4,'kv'=4,'tp'=2] {'tp'}, dimensions={0} | all-to-all | bytes 65536 | tf_op jit(solution)/shard_map/all_to_all | solution.py:30
  12.0 15.1 %all_gather.12 = bf16[32,2048]{1,0:T(8,128)(2,1)S(1)} all-gather(bf16[32,512]{1,0:T(8,128)(2,1)S(1)} %bitcast.140), channel_id=1, replica_groups=mesh['dp'=4,'kv'=4,'tp'=2] {'kv'}, dimensions={1}, use_global_device_ids=true | all-gather | bytes 163840 | tf_op jit(solution)/shard_map/all_gather | solution.py:32
  27.2 3.7 %convolution_multiply_fusion.3 = f32[32,1408]{1,0:T(8,128)S(1)} fusion(bf16[2048,1408]{1,0:T(8,128)(2,1)} %param.24, bf16[32,2048]{1,0:T(8,128)(2,1)S(1)} %all_gather.12, f32[2048]{0:T(1024)} %param.23, f32[32]{0:T(128)S(1)} %add_rsqrt_fusion.5), kind=kOutput, calls=%fused_computation.5 | convolution fusion | flops 184791040 | bytes 6086784 | tf_op jit(solution)/shard_map/dot_general | solution.py:16
  31.0 7.1 %fusion.21 = f32[32,2048]{1,0:T(8,128)} fusion(bf16[1408,2048]{1,0:T(8,128)(2,1)} %param.26, bf16[2048,1408]{1,0:T(8,128)(2,1)} %param.25, f32[32,1408]{1,0:T(8,128)S(1)} %convolution_multiply_fusion.3, bf16[32,2048]{1,0:T(8,128)(2,1)S(1)} %all_gather.12, f32[2048]{0:T(1024)S(1)} %copy-done.4, f32[32]{0:T(128)S(1)} %add_rsqrt_fusion.5), kind=kOutput, calls=%fused_computation.41 | convolution fusion | flops 369610752 | bytes 12116096 | tf_op jit(solution)/shard_map/dot_general | solution.py:25
  38.9 20.5 %reduce-scatter.3.cloned.1.call-done = f32[32,512]{1,0:T(8,128)} async-done(((f32[32,2048]{1,0:T(8,128)}), f32[32,512]{1,0:T(8,128)}) %reduce-scatter.3.cloned.1.call-update) | async-done | bytes 65552 | tf_op jit(solution)/shard_map/reduce_scatter | solution.py:35
  60.2 3.8 %all_to_all.58 = f32[2,32,256]{2,1,0:T(8,128)S(1)} all-to-all(f32[2,32,256]{2,1,0:T(8,128)S(1)} %pad_maximum_fusion.1), channel_id=1, replica_groups=mesh['dp'=4,'kv'=4,'tp'=2] {'tp'}, dimensions={0} | all-to-all | bytes 131072 | tf_op jit(solution)/shard_map/all_to_all | solution.py:37
  64.0 14.3 %all_gather.13 = bf16[64,2048]{1,0:T(8,128)(2,1)S(1)} all-gather(bf16[64,256]{1,0:T(8,128)(2,1)S(1)} %fusion.51), channel_id=1, replica_groups=mesh['dp'=4,'kv'=4,'tp'=2] {'kv','tp'}, dimensions={1}, use_global_device_ids=true | all-gather | bytes 294912 | tf_op jit(solution)/shard_map/all_gather | solution.py:119
  79.1 1.5 fusion.10
  80.7 1.5 fusion.9
  83.0 3.4 %all-to-all-start.2 = ((bf16[4,64,256]{2,0,1:T(4,128)(2,1)}), bf16[4,64,256]{2,0,1:T(4,128)(2,1)S(1)}, u32[]{:S(2)}, u32[]{:S(2)}) async-start(bf16[4,64,256]{2,0,1:T(4,128)(2,1)} %copy.88), calls=%async_computation.3 | async-start | bytes 262144 | tf_op jit(solution)/shard_map/all_to_all | solution.py:127
  86.7 0.9 fusion.80
  87.8 5.3 %all-to-all-done.2 = bf16[4,64,256]{2,0,1:T(4,128)(2,1)S(1)} async-done(((bf16[4,64,256]{2,0,1:T(4,128)(2,1)}), bf16[4,64,256]{2,0,1:T(4,128)(2,1)S(1)}, u32[]{:S(2)}, u32[]{:S(2)}) %all-to-all-start.2) | async-done | bytes 131104 | tf_op jit(solution)/shard_map/all_to_all | solution.py:127
  95.9 1.0 convolution_bitcast_fusion.3
  96.9 1.0 fusion.7
  98.5 14.2 %all_gather.14 = bf16[64,2048]{1,0:T(8,128)(2,1)S(1)} all-gather(bf16[8,2048]{1,0:T(8,128)(2,1)S(1)} %fusion.70), channel_id=1, replica_groups=mesh['dp'=4,'kv'=4,'tp'=2] {'kv','tp'}, dimensions={0}, use_global_device_ids=true | all-gather | bytes 294912 | tf_op jit(solution)/shard_map/all_gather | solution.py:150
  112.7 1.2 convolution_convert_fusion
  113.9 1.2 convolution_convert_fusion.1
  115.2 3.7 %all_to_all.59 = bf16[2,32,256]{2,1,0:T(8,128)(2,1)S(1)} all-to-all(bf16[2,32,256]{2,1,0:T(8,128)(2,1)S(1)} %bitcast.139), channel_id=1, replica_groups=mesh['dp'=4,'kv'=4,'tp'=2] {'tp'}, dimensions={0} | all-to-all | bytes 65536 | tf_op jit(solution)/shard_map/all_to_all | solution.py:30
  119.0 13.6 %all_gather.15 = bf16[32,2048]{1,0:T(8,128)(2,1)S(1)} all-gather(bf16[32,512]{1,0:T(8,128)(2,1)S(1)} %bitcast.141), channel_id=1, replica_groups=mesh['dp'=4,'kv'=4,'tp'=2] {'kv'}, dimensions={1}, use_global_device_ids=true | all-gather | bytes 163840 | tf_op jit(solution)/shard_map/all_gather | solution.py:32
  132.7 3.6 %convolution_multiply_fusion.1 = f32[32,1408]{1,0:T(8,128)S(1)} fusion(bf16[2048,1408]{1,0:T(8,128)(2,1)} %param.37, bf16[32,2048]{1,0:T(8,128)(2,1)S(1)} %all_gather.15, f32[2048]{0:T(1024)S(1)} %copy-done.5, f32[32]{0:T(128)S(1)} %add_rsqrt_fusion.3), kind=kOutput, calls=%fused_computation.2 | convolution fusion | flops 184791040 | bytes 6086784 | tf_op jit(solution)/shard_map/dot_general | solution.py:16
  136.3 7.0 %fusion.20 = f32[32,2048]{1,0:T(8,128)} fusion(bf16[1408,2048]{1,0:T(8,128)(2,1)} %param.39, bf16[2048,1408]{1,0:T(8,128)(2,1)} %param.38, f32[32,1408]{1,0:T(8,128)S(1)} %convolution_multiply_fusion.1, bf16[32,2048]{1,0:T(8,128)(2,1)S(1)} %all_gather.15, f32[2048]{0:T(1024)S(1)} %copy-done.5, f32[32]{0:T(128)S(1)} %add_rsqrt_fusion.3), kind=kOutput, calls=%fused_computation.40 | convolution fusion | flops 369610752 | bytes 12116096 | tf_op jit(solution)/shard_map/dot_general | solution.py:25
  143.4 2.8 %fusion.4 = f32[1,16,128,128]{3,2,1,0:T(8,128)} fusion(f32[8,16,128]{2,0,1:T(8,128)S(1)} %fusion.7, f32[1,16,128,128]{3,2,1,0:T(8,128)S(1)} %copy-done.1, f32[16]{0:T(128)S(1)} %fusion.86, f32[8,16,128]{2,1,0:T(8,128)S(1)} %get-tuple-element.24), kind=kOutput, calls=%fused_computation.9 | convolution fusion | flops 25690112 | bytes 2228288 | tf_op jit(solution)/shard_map/sthk,sthv->shkv/dot_general | solution.py:85
  146.3 16.4 %reduce-scatter.5.cloned.1.call-done = f32[32,512]{1,0:T(8,128)} async-done(((f32[32,2048]{1,0:T(8,128)}), f32[32,512]{1,0:T(8,128)}) %reduce-scatter.5.cloned.1.call-update) | async-done | bytes 65552 | tf_op jit(solution)/shard_map/reduce_scatter | solution.py:35
  163.4 3.8 %all_to_all.60 = f32[2,32,256]{2,1,0:T(8,128)S(1)} all-to-all(f32[2,32,256]{2,1,0:T(8,128)S(1)} %pad_maximum_fusion.2), channel_id=1, replica_groups=mesh['dp'=4,'kv'=4,'tp'=2] {'tp'}, dimensions={0} | all-to-all | bytes 131072 | tf_op jit(solution)/shard_map/all_to_all | solution.py:37
  (81 shorter events, 8.0 us)
Async XLA Ops:
  7.2 71.4 %copy-start = (bf16[2048,256]{1,0:T(8,128)(2,1)S(1)}, bf16[2048,256]{1,0:T(8,128)(2,1)}, u32[]{:S(2)}) copy-start(bf16[2048,256]{1,0:T(8,128)(2,1)} %param.31) | copy-start | bytes 3145732
  7.2 23.7 %copy-start.4 = (f32[2048]{0:T(1024)S(1)}, f32[2048]{0:T(1024)}, u32[]{:S(2)}) copy-start(f32[2048]{0:T(1024)} %param.23) | copy-start | bytes 24580
  7.2 52.2 %reduce-scatter.3.cloned.1.call-start = ((), (), s32[]{:S(2)}) async-start(), calls=%async_computation.7 | async-start | bytes 327680 | tf_op jit(solution)/shard_map/reduce_scatter | solution.py:35
  30.9 7.9 %copy-start.8 = (f32[16]{0:T(128)S(1)}, f32[16]{0:T(128)}, u32[]{:S(2)}) copy-start(f32[16]{0:T(128)} %param.34) | copy-start | bytes 196
  30.9 33.0 %copy-start.3 = (bf16[64,256]{1,0:T(8,128)(2,1)S(1)}, bf16[64,256]{1,0:T(8,128)(2,1)}, u32[]{:S(2)}) copy-start(bf16[64,256]{1,0:T(8,128)(2,1)} %param.20) | copy-start | bytes 98308
  30.9 47.5 %copy-start.6 = (f32[2048]{0:T(1024)S(1)}, f32[2048]{0:T(1024)}, u32[]{:S(2)}) copy-start(f32[2048]{0:T(1024)} %param.27) | copy-start | bytes 24580
  30.9 47.9 %copy-start.2 = (bf16[2048,256]{1,0:T(8,128)(2,1)S(1)}, bf16[2048,256]{1,0:T(8,128)(2,1)}, u32[]{:S(2)}) copy-start(bf16[2048,256]{1,0:T(8,128)(2,1)} %param.30) | copy-start | bytes 3145732
  38.1 48.3 %copy-start.7 = (bf16[2048,16]{0,1:T(8,128)(2,1)S(1)}, bf16[2048,16]{0,1:T(8,128)(2,1)}, u32[]{:S(2)}) copy-start(bf16[2048,16]{0,1:T(8,128)(2,1)} %param.33) | copy-start | bytes 196612
  64.0 31.9 %copy-start.1 = (f32[1,16,128,128]{3,2,1,0:T(8,128)S(1)}, f32[1,16,128,128]{3,2,1,0:T(8,128)}, u32[]{:S(2)}) copy-start(f32[1,16,128,128]{3,2,1,0:T(8,128)} %param.22) | copy-start | bytes 3145732
  80.7 52.0 %copy-start.5 = (f32[2048]{0:T(1024)S(1)}, f32[2048]{0:T(1024)}, u32[]{:S(2)}) copy-start(f32[2048]{0:T(1024)} %param.36) | copy-start | bytes 24580
  83.0 10.1 %all-to-all-start.2 = ((bf16[4,64,256]{2,0,1:T(4,128)(2,1)}), bf16[4,64,256]{2,0,1:T(4,128)(2,1)S(1)}, u32[]{:S(2)}, u32[]{:S(2)}) async-start(bf16[4,64,256]{2,0,1:T(4,128)(2,1)} %copy.88), calls=%async_computation.3 | async-start | bytes 262144 | tf_op jit(solution)/shard_map/all_to_all | solution.py:127
  86.4 76.3 %reduce-scatter.5.cloned.1.call-start = ((), (), s32[]{:S(2)}) async-start(), calls=%async_computation.8 | async-start | bytes 327680 | tf_op jit(solution)/shard_map/reduce_scatter | solution.py:35
Sparse Core Ops, SparseCore 0:
  38.2 21.0 reduce-scatter.2
  143.5 19.0 reduce-scatter.4
